TPU v7x, 32 devices: a whole 2x2x4 slice. The times are simulated.
32 devices in a mesh: sp: 8 (over z, y), tp: 4 (over x, core).
Axes of the slice: x: 2, y: 2, z: 4, core: 2. Of those that a mesh axis runs over, the one named last changes fastest.
Arguments:
- inputs: bfloat16 [8, 6144, 2048], P(None, ('sp', 'tp')), may hold values from -6 to 6
- norm_gain: bfloat16 [2048], replicated, may hold values from 0.099609375 to 1.8984375
- key_weight: bfloat16 [2048, 512], replicated, may hold values from -0.125 to 0.125
- value_weight: bfloat16 [2048, 512], replicated, may hold values from -0.125 to 0.125
- query: bfloat16 [8, 1024], P('sp', 'tp'), may hold values from -15 to 15
- head_bias: bfloat16 [16], P('tp'), may hold values from -14 to -6
Outputs:
- key_cache: bfloat16 [8, 6144, 512], P('sp', None, 'tp')
- value_cache: bfloat16 [8, 6144, 512], P('sp', None, 'tp')
- first_read: bfloat16 [8, 1024], P('sp', 'tp')
All inputs are finite; a program needn't handle non-finite values.
Results may differ from a plain program's by a relative error of at most 0.012.
Values may be sent and summed in bfloat16 or wider, within the bound.
A program may use at most 128 MiB of HBM per device.

v0:
```python
import jax
import jax.numpy as jnp
from jax import lax
from jax.sharding import PartitionSpec as P

HEAD_DIMENSION = 64
EPSILON = 1e-06


def body(inputs, norm_gain, key_weight, value_weight, query, head_bias):
    groups = lax.axis_size("tp")
    seq_count, span_len, model_width = inputs.shape
    head_cols = key_weight.shape[1] // groups
    kv_heads = head_cols // HEAD_DIMENSION
    q_heads = query.shape[1] // HEAD_DIMENSION
    repeat = q_heads // kv_heads
    widened = inputs.astype(jnp.float32)
    normed = widened * lax.rsqrt(jnp.mean(widened * widened, axis=-1, keepdims=True) + EPSILON)
    normed = (normed * norm_gain.astype(jnp.float32)).astype(jnp.bfloat16)
    key_rows = jnp.einsum(
        "kru,uao->karo",
        normed,
        key_weight.reshape(model_width, groups, head_cols),
        preferred_element_type=jnp.float32,
    ).astype(jnp.bfloat16)
    value_rows = jnp.einsum(
        "kru,uao->karo",
        normed,
        value_weight.reshape(model_width, groups, head_cols),
        preferred_element_type=jnp.float32,
    ).astype(jnp.bfloat16)
    key_cache, value_cache = (
        lax.all_to_all(
            key_rows.reshape(seq_count * groups, span_len, head_cols),
            ("sp", "tp"),
            split_axis=0,
            concat_axis=1,
            tiled=True,
        ),
        lax.all_to_all(
            value_rows.reshape(seq_count * groups, span_len, head_cols),
            ("sp", "tp"),
            split_axis=0,
            concat_axis=1,
            tiled=True,
        ),
    )
    seq_len = key_cache.shape[1]
    query_tensor = query.reshape(kv_heads, repeat, HEAD_DIMENSION)
    key_tensor = key_cache.reshape(seq_len, kv_heads, HEAD_DIMENSION)
    value_tensor = value_cache.reshape(seq_len, kv_heads, HEAD_DIMENSION)
    score_logits = jnp.einsum(
        "ebx,uex->ebu", query_tensor, key_tensor, preferred_element_type=jnp.float32
    )
    score_logits = score_logits * HEAD_DIMENSION ** (-0.5) + head_bias.astype(jnp.float32).reshape(
        kv_heads, repeat, 1
    )
    log_keep = jax.nn.log_sigmoid(-score_logits)
    suffix_logs = lax.cumsum(log_keep, axis=2, reverse=True) - log_keep
    stick_weights = jnp.exp(jax.nn.log_sigmoid(score_logits) + suffix_logs).astype(jnp.bfloat16)
    attended_output = jnp.einsum(
        "euq,qec->euc", stick_weights, value_tensor, preferred_element_type=jnp.float32
    )
    first_read = attended_output.reshape(1, q_heads * HEAD_DIMENSION).astype(jnp.bfloat16)
    return (key_cache, value_cache, first_read)


def solution(mesh):
    placed = (P(None, ("sp", "tp"), None), P(), P(), P(), P("sp", "tp"), P("tp"))
    return jax.shard_map(
        body,
        mesh=mesh,
        in_specs=placed,
        out_specs=(P("sp", None, "tp"), P("sp", None, "tp"), P("sp", "tp")),
        check_vma=False,
    )
```

profile of v0, /device:TPU:0, one launch (start us, length us, event | category | flops | bytes accessed | tf_op | source)
XLA Modules:
  0.0 114.2 jit_solution(8614409717820748399)
XLA Ops:
  0.6 0.0 copy-start
  0.6 0.0 copy-start.1
  0.7 0.0 copy-start.2
  0.7 4.2 %fusion = f32[8,192]{1,0:T(8,128)S(1)} fusion(bf16[8,192,2048]{2,1,0:T(8,128)(2,1)} %param.6), kind=kLoop, calls=%fused_computation.2 | loop fusion | flops 9435648 | bytes 6297600 | tf_op jit(solution)/shard_map/reduce_sum | solution.py:18
  4.9 0.0 copy-done.2
  4.9 0.0 copy-done
  5.0 0.9 copy-done.1
  5.9 4.6 %fusion.12 = bf16[8,192,4,128]{3,1,2,0:T(8,128)(2,1)} fusion(bf16[8,192,2048]{2,1,0:T(8,128)(2,1)S(1)} %copy-done.1, f32[2048]{0:T(1024)S(1)} %convert_element_type.40, f32[8,192]{1,0:T(8,128)S(1)} %add_rsqrt_fusion, bf16[2048,512]{1,0:T(8,128)(2,1)S(1)} %copy-done), kind=kOutput, calls=%fused_computation.15 | convolution fusion | flops 3234594816 | bytes 9975808 | tf_op jit(solution)/shard_map/kru,uao->karo/dot_general | solution.py:20
  10.5 7.4 %all-to-all-start = ((bf16[32,192,128]{2,1,0:T(8,128)(2,1)}), bf16[32,192,128]{2,1,0:T(8,128)(2,1)}, u32[]{:S(2)}, u32[]{:S(2)}) async-start(bf16[32,192,128]{2,1,0:T(8,128)(2,1)} %bitcast.58), calls=%async_computation | async-start | bytes 3145728 | tf_op jit(solution)/shard_map/all_to_all | solution.py:33
  17.9 8.2 %fusion.15 = bf16[8,192,4,128]{3,1,2,0:T(8,128)(2,1)} fusion(bf16[8,192,2048]{2,1,0:T(8,128)(2,1)} %param.6, f32[2048]{0:T(1024)S(1)} %convert_element_type.40, f32[8,192]{1,0:T(8,128)S(1)} %add_rsqrt_fusion, bf16[2048,512]{1,0:T(8,128)(2,1)} %param.9), kind=kOutput, calls=%fused_computation.16 | convolution fusion | flops 3234594816 | bytes 9975808 | tf_op jit(solution)/shard_map/kru,uao->karo/dot_general | solution.py:26
  26.1 0.0 copy-start.3
  26.1 0.0 copy-start.4
  26.1 29.4 %all-to-all-done = bf16[32,192,128]{2,1,0:T(8,128)(2,1)} async-done(((bf16[32,192,128]{2,1,0:T(8,128)(2,1)}), bf16[32,192,128]{2,1,0:T(8,128)(2,1)}, u32[]{:S(2)}, u32[]{:S(2)}) %all-to-all-start) | async-done | bytes 1572896 | tf_op jit(solution)/shard_map/all_to_all | solution.py:33
  55.6 4.1 %all-to-all-start.1 = ((bf16[32,192,128]{2,1,0:T(8,128)(2,1)}), bf16[32,192,128]{2,1,0:T(8,128)(2,1)}, u32[]{:S(2)}, u32[]{:S(2)}) async-start(bf16[32,192,128]{2,1,0:T(8,128)(2,1)} %bitcast.57), calls=%async_computation.1 | async-start | bytes 3145728 | tf_op jit(solution)/shard_map/all_to_all | solution.py:40
  59.7 0.0 copy-done.3
  59.7 0.1 reshape.75
  59.8 0.0 copy-done.4
  59.8 0.1 reshape.79
  59.9 4.5 %copy.21 = bf16[32,192,128]{1,0,2:T(8,128)(2,1)} copy(bf16[32,192,128]{2,1,0:T(8,128)(2,1)} %all-to-all-done) | data formatting | bytes 3145728 | tf_op jit(solution)/shard_map/all_to_all | solution.py:33
  64.4 4.5 %reshape.74 = bf16[6144,2,64]{0,2,1:T(8,128)(2,1)} reshape(bf16[32,192,128]{1,0,2:T(8,128)(2,1)} %copy.21) | data formatting | bytes 3145728 | tf_op jit(solution)/shard_map/reshape | solution.py:50
  68.9 1.8 %fusion.21 = (f32[2,2,6144]{2,1,0:T(2,128)S(1)}, f32[2,2,6144]{2,1,0:T(2,128)S(1)}) fusion(f32[2,2]{1,0:T(2,128)S(1)} %reshape.79, bf16[6144,2,64]{0,2,1:T(8,128)(2,1)} %reshape.74, bf16[2,2,64]{2,1,0:T(2,128)(2,1)S(1)} %reshape.75), kind=kOutput, calls=%fused_computation.23 | convolution fusion | flops 3366912 | bytes 1770000 | tf_op jit(solution)/shard_map/ebx,uex->ebu/dot_general | solution.py:52
  70.7 0.1 reshape.76
  70.8 5.0 %reduce-window.6 = f32[2,2,48,128]{3,2,1,0:T(8,128)S(1)} reduce-window(f32[2,2,48,128]{3,2,1,0:T(8,128)S(1)} %reshape.76, f32[]{:T(128)} %constant.6.clone.1), window={size=1x1x1x128 pad=0_0x0_0x0_0x0_127}, to_apply=%region_1.2 | reduce-window | flops 3121152 | bytes 196612 | tf_op jit(solution)/shard_map/reduce-window
  75.9 0.1 slice_reduce_fusion
  76.0 0.7 reduce-window.9
  76.6 0.1 slice.9
  76.7 0.1 broadcast_add_fusion
  76.8 0.1 reduce_window_sum.15
  76.9 20.3 %all-to-all-done.1 = bf16[32,192,128]{2,1,0:T(8,128)(2,1)} async-done(((bf16[32,192,128]{2,1,0:T(8,128)(2,1)}), bf16[32,192,128]{2,1,0:T(8,128)(2,1)}, u32[]{:S(2)}, u32[]{:S(2)}) %all-to-all-start.1) | async-done | bytes 1572896 | tf_op jit(solution)/shard_map/all_to_all | solution.py:40
  97.2 4.5 %copy.22 = bf16[32,192,128]{1,0,2:T(8,128)(2,1)} copy(bf16[32,192,128]{2,1,0:T(8,128)(2,1)} %all-to-all-done.1) | data formatting | bytes 3145728 | tf_op jit(solution)/shard_map/all_to_all | solution.py:40
  101.7 4.5 %reshape.78 = bf16[6144,2,64]{0,2,1:T(8,128)(2,1)} reshape(bf16[32,192,128]{1,0,2:T(8,128)(2,1)} %copy.22) | data formatting | bytes 3145728 | tf_op jit(solution)/shard_map/reshape | solution.py:51
  106.2 2.1 %convolution_convert_fusion = bf16[2,2,64]{2,1,0:T(2,128)(2,1)S(1)} fusion(bf16[6144,2,64]{0,2,1:T(8,128)(2,1)} %reshape.78, f32[2,2,6144]{2,1,0:T(2,128)S(1)} %reduce_window_sum.15, f32[2,2,6144]{2,1,0:T(2,128)S(1)} %get-tuple-element.4), kind=kOutput, calls=%fused_computation.17 | convolution fusion | flops 3588352 | bytes 1769984 | tf_op jit(solution)/shard_map/euq,qec->euc/dot_general | solution.py:61
  108.3 0.7 convert_element_type.48
  108.9 2.7 %copy.40 = bf16[1,6144,128]{2,1,0:T(8,128)(2,1)} copy(bf16[1,6144,128]{2,1,0:T(8,128)(2,1)} %bitcast.5) | data formatting | bytes 3145728
  111.6 2.7 %copy.41 = bf16[1,6144,128]{2,1,0:T(8,128)(2,1)} copy(bf16[1,6144,128]{2,1,0:T(8,128)(2,1)} %bitcast.10) | data formatting | bytes 3145728
  (3 shorter events, 0.0 us)
Async XLA Ops:
  0.6 4.3 %copy-start = (bf16[2048,512]{1,0:T(8,128)(2,1)S(1)}, bf16[2048,512]{1,0:T(8,128)(2,1)}, u32[]{:S(2)}) copy-start(bf16[2048,512]{1,0:T(8,128)(2,1)} %param.8) | copy-start | bytes 6291460
  0.6 5.2 %copy-start.1 = (bf16[8,192,2048]{2,1,0:T(8,128)(2,1)S(1)}, bf16[8,192,2048]{2,1,0:T(8,128)(2,1)}, u32[]{:S(2)}) copy-start(bf16[8,192,2048]{2,1,0:T(8,128)(2,1)} %param.6) | copy-start | bytes 18874372
  0.7 4.3 %copy-start.2 = (bf16[2048]{0:T(1024)(128)(2,1)S(1)}, bf16[2048]{0:T(1024)(128)(2,1)}, u32[]{:S(2)}) copy-start(bf16[2048]{0:T(1024)(128)(2,1)} %param.7) | copy-start | bytes 12292
  10.5 45.1 %all-to-all-start = ((bf16[32,192,128]{2,1,0:T(8,128)(2,1)}), bf16[32,192,128]{2,1,0:T(8,128)(2,1)}, u32[]{:S(2)}, u32[]{:S(2)}) async-start(bf16[32,192,128]{2,1,0:T(8,128)(2,1)} %bitcast.58), calls=%async_computation | async-start | bytes 3145728 | tf_op jit(solution)/shard_map/all_to_all | solution.py:33
  26.1 33.5 %copy-start.3 = (bf16[1,256]{1,0:T(2,128)(2,1)S(1)}, bf16[1,256]{1,0:T(2,128)(2,1)}, u32[]{:S(2)}) copy-start(bf16[1,256]{1,0:T(2,128)(2,1)} %param.10) | copy-start | bytes 1540
  26.1 33.7 %copy-start.4 = (bf16[4]{0:T(256)(128)(2,1)S(1)}, bf16[4]{0:T(256)(128)(2,1)}, u32[]{:S(2)}) copy-start(bf16[4]{0:T(256)(128)(2,1)} %param.11) | copy-start | bytes 28
  55.6 41.6 %all-to-all-start.1 = ((bf16[32,192,128]{2,1,0:T(8,128)(2,1)}), bf16[32,192,128]{2,1,0:T(8,128)(2,1)}, u32[]{:S(2)}, u32[]{:S(2)}) async-start(bf16[32,192,128]{2,1,0:T(8,128)(2,1)} %bitcast.57), calls=%async_computation.1 | async-start | bytes 3145728 | tf_op jit(solution)/shard_map/all_to_all | solution.py:40
where the time goes:
time: 115 us; the launch traced here: 114 us
  waiting for transfers between devices  49.8 us (43%)
  local copies, waits for them, and re-layouts  25.4 us (22%)
  matrix products  16.7 us (15%)
  starting transfers between devices  11.5 us (10%)
  other arithmetic  10.1 us (9%)
    all_to_all x1, waiting for transfers between devices, body(): lax.all_to_all(key_rows.reshape(seq_count * groups, span_len, head_cols),...  29.4 us
    all_to_all x1, waiting for transfers between devices, body(): lax.all_to_all(value_rows.reshape(seq_count * groups, span_len, head_cols...  20.3 us
    dot_general x1, matrix products, body(): jnp.einsum('kru,uao->karo', normed, value_weight.reshape(model_width, gro...  8.19 us
    all_to_all x1, starting transfers between devices, body(): lax.all_to_all(key_rows.reshape(seq_count * groups, span_len, head_cols),...  7.43 us
    unnamed x12, local copies, waits for them, and re-layouts  6.27 us
    another operation x2, other arithmetic  5.69 us
    dot_general x1, matrix products, body(): jnp.einsum('kru,uao->karo', normed, key_weight.reshape(model_width, group...  4.62 us
    all_to_all x1, local copies, waits for them, and re-layouts, body(): lax.all_to_all(key_rows.reshape(seq_count * groups, span_len, head_cols),...  4.53 us
  transfers between devices with their start and end apart: 2, of which 2 were waited for; matrix products, arithmetic and copies ran while one was open for 22% of the time, Pallas kernels for 0%

commit v1 on v0

--- a/solution.py
+++ b/solution.py
@@ -29,6 +29,15 @@
         value_weight.reshape(model_width, groups, head_cols),
         preferred_element_type=jnp.float32,
     ).astype(jnp.bfloat16)
+    run_sites_for = lambda u_in, bus_axis: jnp.concatenate(
+        lax.all_to_all(
+            jnp.stack(jnp.split(u_in, lax.axis_size(bus_axis), axis=0), axis=0),
+            bus_axis,
+            split_axis=0,
+            concat_axis=0,
+        ),
+        axis=1,
+    )
     key_cache, value_cache = (
         lax.all_to_all(
             key_rows.reshape(seq_count * groups, span_len, head_cols),
@@ -37,13 +46,7 @@
             concat_axis=1,
             tiled=True,
         ),
-        lax.all_to_all(
-            value_rows.reshape(seq_count * groups, span_len, head_cols),
-            ("sp", "tp"),
-            split_axis=0,
-            concat_axis=1,
-            tiled=True,
-        ),
+        run_sites_for(value_rows.reshape(seq_count * groups, span_len, head_cols), ("sp", "tp")),
     )
     seq_len = key_cache.shape[1]
     query_tensor = query.reshape(kv_heads, repeat, HEAD_DIMENSION)

time: 115 us -> 142 us (1.23)
  local copies, waits for them, and re-layouts: 25.4 us -> 45.4 us
  waiting for transfers between devices: 49.8 us -> 57.7 us
    unnamed x12 -> x43, local copies, waits for them, and re-layouts: 6.27 us -> 25.6 us
    all_to_all x1, waiting for transfers between devices: 20.3 us -> 29.4 us  [body(): lax.all_to_all(jnp.stack(jnp.split(u_in, lax.axis_size(bus_axis), axis=0)...]
    another operation x1 -> x3, local copies, waits for them, and re-layouts: 0.08 us -> 5.18 us  [the longest x1 4.49 us: body(): value_tensor = value_cache.reshape(seq_len, kv_heads, HEAD_DIMENSION)]
    reshape x2 -> x1, local copies, waits for them, and re-layouts: 4.57 us -> 0.08 us  [the longest x1 4.49 us: body(): value_tensor = value_cache.reshape(seq_len, kv_heads, HEAD_DIMENSION)]
    dot_general x1, matrix products: 8.19 us -> 3.73 us  [body(): jnp.einsum('kru,uao->karo', normed, value_weight.reshape(model_width, gro...]
    dot_general x1, matrix products: 4.62 us -> 8.19 us  [body(): jnp.einsum('kru,uao->karo', normed, key_weight.reshape(model_width, group...]
    all_to_all x1, starting transfers between devices: 4.1 us -> 7.43 us  [body(): lax.all_to_all(jnp.stack(jnp.split(u_in, lax.axis_size(bus_axis), axis=0)...]
    all_to_all x1, starting transfers between devices: 7.43 us -> 4.1 us  [body(): lax.all_to_all(key_rows.reshape(seq_count * groups, span_len, head_cols),...]
  transfers between devices with their start and end apart: 2 -> 2, of which waited for: 2 -> 2; matrix products, arithmetic and copies ran while one was open for 22% -> 12% of each run, Pallas kernels for 0% -> 0%
where the time goes in v1:
time: 142 us; the launch traced here: 141 us
  waiting for transfers between devices  57.7 us (41%)
  local copies, waits for them, and re-layouts  45.4 us (32%)
  matrix products  15.8 us (11%)
  starting transfers between devices  11.5 us (8%)
  other arithmetic  10.1 us (7%)
    all_to_all x1, waiting for transfers between devices, body(): lax.all_to_all(jnp.stack(jnp.split(u_in, lax.axis_size(bus_axis), axis=0)...  29.4 us
    all_to_all x1, waiting for transfers between devices, body(): lax.all_to_all(key_rows.reshape(seq_count * groups, span_len, head_cols),...  28.3 us
    unnamed x43, local copies, waits for them, and re-layouts  25.6 us
    dot_general x1, matrix products, body(): jnp.einsum('kru,uao->karo', normed, key_weight.reshape(model_width, group...  8.19 us
    all_to_all x1, starting transfers between devices, body(): lax.all_to_all(jnp.stack(jnp.split(u_in, lax.axis_size(bus_axis), axis=0)...  7.43 us
    another operation x2, other arithmetic  5.69 us
    all_to_all x1, local copies, waits for them, and re-layouts, body(): lax.all_to_all(jnp.stack(jnp.split(u_in, lax.axis_size(bus_axis), axis=0)...  4.53 us
    all_to_all x1, local copies, waits for them, and re-layouts, body(): lax.all_to_all(key_rows.reshape(seq_count * groups, span_len, head_cols),...  4.53 us
  transfers between devices with their start and end apart: 2, of which 2 were waited for; matrix products, arithmetic and copies ran while one was open for 12% of the time, Pallas kernels for 0%

profile of v1, /device:TPU:0, one launch (start us, length us, event | category | flops | bytes accessed | tf_op | source)
XLA Modules:
  0.0 141.3 jit_solution(17634408036178562669)
XLA Ops:
  0.6 0.0 copy-start
  0.6 0.0 copy-start.1
  0.7 0.0 copy-start.2
  0.7 4.2 %fusion = f32[8,192]{1,0:T(8,128)S(1)} fusion(bf16[8,192,2048]{2,1,0:T(8,128)(2,1)} %param.6), kind=kLoop, calls=%fused_computation.2 | loop fusion | flops 9435648 | bytes 6297600 | tf_op jit(solution)/shard_map/reduce_sum | solution.py:18
  4.9 0.0 copy-done.2
  4.9 0.0 copy-done
  5.0 0.9 copy-done.1
  5.9 3.7 %fusion.15 = bf16[8,192,4,128]{3,1,2,0:T(8,128)(2,1)S(1)} fusion(bf16[8,192,2048]{2,1,0:T(8,128)(2,1)S(1)} %copy-done.1, f32[2048]{0:T(1024)S(1)} %convert_element_type.40, f32[8,192]{1,0:T(8,128)S(1)} %add_rsqrt_fusion, bf16[2048,512]{1,0:T(8,128)(2,1)S(1)} %copy-done), kind=kOutput, calls=%fused_computation.16 | convolution fusion | flops 3234594816 | bytes 9975808 | tf_op jit(solution)/shard_map/kru,uao->karo/dot_general | solution.py:26
  9.6 0.6 constant_dynamic-update-slice_fusion.31
  10.3 0.6 constant_dynamic-update-slice_fusion.30
  10.9 0.6 constant_dynamic-update-slice_fusion.29
  11.5 0.6 constant_dynamic-update-slice_fusion.28
  12.1 0.6 constant_dynamic-update-slice_fusion.27
  12.7 0.6 constant_dynamic-update-slice_fusion.26
  13.4 0.6 constant_dynamic-update-slice_fusion.25
  14.0 0.6 constant_dynamic-update-slice_fusion.24
  14.6 0.6 constant_dynamic-update-slice_fusion.23
  15.2 0.6 constant_dynamic-update-slice_fusion.22
  15.9 0.6 constant_dynamic-update-slice_fusion.21
  16.5 0.6 constant_dynamic-update-slice_fusion.20
  17.1 0.6 constant_dynamic-update-slice_fusion.19
  17.7 0.6 constant_dynamic-update-slice_fusion.18
  18.4 0.6 constant_dynamic-update-slice_fusion.17
  19.0 0.6 constant_dynamic-update-slice_fusion.16
  19.6 0.6 constant_dynamic-update-slice_fusion.15
  20.2 0.6 constant_dynamic-update-slice_fusion.14
  20.9 0.6 constant_dynamic-update-slice_fusion.13
  21.5 0.6 constant_dynamic-update-slice_fusion.12
  22.1 0.6 constant_dynamic-update-slice_fusion.11
  22.7 0.6 constant_dynamic-update-slice_fusion.10
  23.3 0.6 constant_dynamic-update-slice_fusion.9
  24.0 0.6 constant_dynamic-update-slice_fusion.8
  24.6 0.6 constant_dynamic-update-slice_fusion.7
  25.2 0.6 constant_dynamic-update-slice_fusion.6
  25.8 0.6 constant_dynamic-update-slice_fusion.5
  26.5 0.6 constant_dynamic-update-slice_fusion.4
  27.1 0.6 constant_dynamic-update-slice_fusion.3
  27.7 0.6 constant_dynamic-update-slice_fusion.2
  28.3 0.6 constant_dynamic-update-slice_fusion.1
  29.0 0.6 constant_dynamic-update-slice_fusion
  29.6 7.4 %all-to-all-start.1 = ((bf16[32,1,192,128]{3,2,1,0:T(8,128)(2,1)}), bf16[32,1,192,128]{3,2,1,0:T(8,128)(2,1)}, u32[]{:S(2)}, u32[]{:S(2)}) async-start(bf16[32,1,192,128]{3,2,1,0:T(8,128)(2,1)} %constant_dynamic-update-slice_fusion), calls=%async_computation.1 | async-start | bytes 3145728 | tf_op jit(solution)/shard_map/all_to_all | solution.py:33
  37.0 8.2 %fusion.12 = bf16[8,192,4,128]{3,1,2,0:T(8,128)(2,1)} fusion(bf16[8,192,2048]{2,1,0:T(8,128)(2,1)} %param.6, f32[2048]{0:T(1024)S(1)} %convert_element_type.40, f32[8,192]{1,0:T(8,128)S(1)} %add_rsqrt_fusion, bf16[2048,512]{1,0:T(8,128)(2,1)} %param.8), kind=kOutput, calls=%fused_computation.15 | convolution fusion | flops 3234594816 | bytes 9975808 | tf_op jit(solution)/shard_map/kru,uao->karo/dot_general | solution.py:20
  45.2 29.4 %all-to-all-done.1 = bf16[32,1,192,128]{3,2,1,0:T(8,128)(2,1)} async-done(((bf16[32,1,192,128]{3,2,1,0:T(8,128)(2,1)}), bf16[32,1,192,128]{3,2,1,0:T(8,128)(2,1)}, u32[]{:S(2)}, u32[]{:S(2)}) %all-to-all-start.1) | async-done | bytes 1572896 | tf_op jit(solution)/shard_map/all_to_all | solution.py:33
  74.7 4.1 %all-to-all-start = ((bf16[32,192,128]{2,1,0:T(8,128)(2,1)}), bf16[32,192,128]{2,1,0:T(8,128)(2,1)}, u32[]{:S(2)}, u32[]{:S(2)}) async-start(bf16[32,192,128]{2,1,0:T(8,128)(2,1)} %bitcast.187), calls=%async_computation | async-start | bytes 3145728 | tf_op jit(solution)/shard_map/all_to_all | solution.py:42
  78.8 0.1 reshape.72
  78.9 0.0 copy-done.4
  78.9 0.1 reshape.75
  79.0 4.5 %copy.58 = bf16[32,1,192,128]{2,0,3,1:T(8,128)(2,1)} copy(bf16[32,1,192,128]{3,2,1,0:T(8,128)(2,1)} %all-to-all-done.1) | data formatting | bytes 3145728 | tf_op jit(solution)/shard_map/all_to_all | solution.py:33
  83.5 4.5 %reshape_reshape.3 = bf16[6144,2,64]{0,2,1:T(8,128)(2,1)} reshape(bf16[32,1,192,128]{2,0,3,1:T(8,128)(2,1)} %copy.58) | data formatting | bytes 3145728 | tf_op jit(solution)/shard_map/reshape;reshape | solution.py:54
  88.0 28.3 %all-to-all-done = bf16[32,192,128]{2,1,0:T(8,128)(2,1)} async-done(((bf16[32,192,128]{2,1,0:T(8,128)(2,1)}), bf16[32,192,128]{2,1,0:T(8,128)(2,1)}, u32[]{:S(2)}, u32[]{:S(2)}) %all-to-all-start) | async-done | bytes 1572896 | tf_op jit(solution)/shard_map/all_to_all | solution.py:42
  116.3 4.5 %copy.57 = bf16[32,192,128]{1,0,2:T(8,128)(2,1)} copy(bf16[32,192,128]{2,1,0:T(8,128)(2,1)} %all-to-all-done) | data formatting | bytes 3145728 | tf_op jit(solution)/shard_map/all_to_all | solution.py:42
  120.8 4.5 %reshape.71 = bf16[6144,2,64]{0,2,1:T(8,128)(2,1)} reshape(bf16[32,192,128]{1,0,2:T(8,128)(2,1)} %copy.57) | data formatting | bytes 3145728 | tf_op jit(solution)/shard_map/reshape | solution.py:53
  125.3 1.8 %fusion.21 = (f32[2,2,6144]{2,1,0:T(2,128)S(1)}, f32[2,2,6144]{2,1,0:T(2,128)S(1)}) fusion(f32[2,2]{1,0:T(2,128)S(1)} %reshape.75, bf16[6144,2,64]{0,2,1:T(8,128)(2,1)} %reshape.71, bf16[2,2,64]{2,1,0:T(2,128)(2,1)S(1)} %reshape.72), kind=kOutput, calls=%fused_computation.23 | convolution fusion | flops 3366912 | bytes 1770000 | tf_op jit(solution)/shard_map/ebx,uex->ebu/dot_general | solution.py:55
  127.1 0.1 reshape.73
  127.2 5.0 %reduce-window.6 = f32[2,2,48,128]{3,2,1,0:T(8,128)S(1)} reduce-window(f32[2,2,48,128]{3,2,1,0:T(8,128)S(1)} %reshape.73, f32[]{:T(128)} %constant.6.clone.1), window={size=1x1x1x128 pad=0_0x0_0x0_0x0_127}, to_apply=%region_1.2 | reduce-window | flops 3121152 | bytes 196612 | tf_op jit(solution)/shard_map/reduce-window
  132.2 0.1 slice_reduce_fusion
  132.3 0.7 reduce-window.9
  133.0 0.1 slice.9
  133.1 0.1 broadcast_add_fusion
  133.2 0.1 reduce_window_sum.15
  133.2 2.1 %convolution_convert_fusion = bf16[2,2,64]{2,1,0:T(2,128)(2,1)S(1)} fusion(bf16[6144,2,64]{0,2,1:T(8,128)(2,1)} %reshape_reshape.3, f32[2,2,6144]{2,1,0:T(2,128)S(1)} %reduce_window_sum.15, f32[2,2,6144]{2,1,0:T(2,128)S(1)} %get-tuple-element.4), kind=kOutput, calls=%fused_computation.17 | convolution fusion | flops 3588352 | bytes 1769984 | tf_op jit(solution)/shard_map/euq,qec->euc/dot_general | solution.py:64
  135.3 0.7 convert_element_type.48
  136.0 2.7 %copy.107 = bf16[1,6144,128]{2,1,0:T(8,128)(2,1)} copy(bf16[1,6144,128]{2,1,0:T(8,128)(2,1)} %bitcast.5) | data formatting | bytes 3145728
  138.6 2.7 %copy.108 = bf16[1,6144,128]{2,1,0:T(8,128)(2,1)} copy(bf16[1,6144,128]{2,1,0:T(8,128)(2,1)} %bitcast.43) | data formatting | bytes 3145728
  (6 shorter events, 0.0 us)
Async XLA Ops:
  0.6 4.3 %copy-start = (bf16[2048,512]{1,0:T(8,128)(2,1)S(1)}, bf16[2048,512]{1,0:T(8,128)(2,1)}, u32[]{:S(2)}) copy-start(bf16[2048,512]{1,0:T(8,128)(2,1)} %param.9) | copy-start | bytes 6291460
  0.6 5.2 %copy-start.1 = (bf16[8,192,2048]{2,1,0:T(8,128)(2,1)S(1)}, bf16[8,192,2048]{2,1,0:T(8,128)(2,1)}, u32[]{:S(2)}) copy-start(bf16[8,192,2048]{2,1,0:T(8,128)(2,1)} %param.6) | copy-start | bytes 18874372
  0.7 4.3 %copy-start.2 = (bf16[2048]{0:T(1024)(128)(2,1)S(1)}, bf16[2048]{0:T(1024)(128)(2,1)}, u32[]{:S(2)}) copy-start(bf16[2048]{0:T(1024)(128)(2,1)} %param.7) | copy-start | bytes 12292
  29.6 45.1 %all-to-all-start.1 = ((bf16[32,1,192,128]{3,2,1,0:T(8,128)(2,1)}), bf16[32,1,192,128]{3,2,1,0:T(8,128)(2,1)}, u32[]{:S(2)}, u32[]{:S(2)}) async-start(bf16[32,1,192,128]{3,2,1,0:T(8,128)(2,1)} %constant_dynamic-update-slice_fusion), calls=%async_computation.1 | async-start | bytes 3145728 | tf_op jit(solution)/shard_map/all_to_all | solution.py:33
  74.7 4.1 %copy-start.3 = (bf16[1,256]{1,0:T(2,128)(2,1)S(1)}, bf16[1,256]{1,0:T(2,128)(2,1)}, u32[]{:S(2)}) copy-start(bf16[1,256]{1,0:T(2,128)(2,1)} %param.10) | copy-start | bytes 1540
  74.7 4.2 %copy-start.4 = (bf16[4]{0:T(256)(128)(2,1)S(1)}, bf16[4]{0:T(256)(128)(2,1)}, u32[]{:S(2)}) copy-start(bf16[4]{0:T(256)(128)(2,1)} %param.11) | copy-start | bytes 28
  74.7 41.6 %all-to-all-start = ((bf16[32,192,128]{2,1,0:T(8,128)(2,1)}), bf16[32,192,128]{2,1,0:T(8,128)(2,1)}, u32[]{:S(2)}, u32[]{:S(2)}) async-start(bf16[32,192,128]{2,1,0:T(8,128)(2,1)} %bitcast.187), calls=%async_computation | async-start | bytes 3145728 | tf_op jit(solution)/shard_map/all_to_all | solution.py:42
